TPU v7x, 1024 devices: a whole 4x8x16 slice. The times are simulated.
1024 devices in a mesh: rep: 2 (over z_hi), fs: 64 (over z_lo, y), tp: 8 (over x, core).
Axes of the slice: x: 4, y: 8, z: 16 (z_hi: 2, z_lo: 8; z = z_hi * 8 + z_lo), core: 2. Of those that a mesh axis runs over, the one named last changes fastest.
Arguments:
- stream: bfloat16 [32768, 1536], P(('rep', 'fs')), may hold values from -6 to 6
- mix_pre_gain: float32 [1536], replicated, may hold values from 0.1 to 1.9
- w_outer_gate: bfloat16 [1536, 768], P('fs', 'tp'), may hold values from -0.15625 to 0.15625
- w_inner_gate: bfloat16 [1536, 768], P('fs', 'tp'), may hold values from -0.15625 to 0.15625
- w_value: bfloat16 [1536, 768], P('fs', 'tp'), may hold values from -0.15625 to 0.15625
- mix_taps: float32 [3, 768], P(None, 'tp'), may hold values from -3 to 3
- w_mix_out: bfloat16 [768, 1536], P('tp', 'fs'), may hold values from -0.625 to 0.625
- mix_post_gain: float32 [1536], replicated, may hold values from 0.1 to 1.9
- ffn_pre_gain: float32 [1536], replicated, may hold values from 0.1 to 1.9
- w_linear: bfloat16 [1536, 4224], P('fs', 'tp'), may hold values from -0.15625 to 0.15625
- w_gated: bfloat16 [1536, 4224], P('fs', 'tp'), may hold values from -0.15625 to 0.15625
- ffn_taps: float32 [3, 4224], P(None, 'tp'), may hold values from -3 to 3
- ffn_bias: float32 [4224], P('tp'), may hold values from -3 to 3
- w_down: bfloat16 [4224, 1536], P('tp', 'fs'), may hold values from -0.25 to 0.25
- ffn_post_gain: float32 [1536], replicated, may hold values from 0.1 to 1.9
Outputs:
- result: bfloat16 [32768, 1536], P(('rep', 'fs'))
All inputs are finite; a program needn't handle non-finite values.
Results may differ from a plain program's by a relative error of at most 0.023.
Values may be sent and summed in bfloat16 or wider, within the bound.
No kernel may reach another device: no remote copies, remote signals or barrier semaphores. Data moves between devices by JAX's collectives and lax.ppermute only.
A program may use at most 64 MiB of HBM per device.

v0:
```python
import jax
import jax.numpy as jnp
from jax import lax
from jax.sharding import Mesh
from jax.sharding import PartitionSpec as P

SEQ_LEN = 128
FS = ("fs_0", "fs_1")
REP_FS = ("rep", "fs_0", "fs_1")


EPS = 1e-06


def in_blocks(x, dim, length):
    before, after = (x.shape[:dim], x.shape[dim + 1 :])
    return jnp.moveaxis(x.reshape(*before, length, -1, *after), dim, 0)


def summed_on_arrival(x, axis, dim):
    tiles = in_blocks(x, dim, lax.axis_size(axis))
    arrived = lax.all_to_all(tiles, axis, split_axis=0, concat_axis=0, tiled=True)
    return arrived.astype(jnp.float32).sum(axis=0)


def sent_to_all(x, axis):
    length = lax.axis_size(axis)
    return lax.all_to_all(jnp.broadcast_to(x[None], (length, *x.shape)), axis, 0, 0, tiled=True)


def of_everyone(x, axis):
    everything = sent_to_all(x, axis)
    return jnp.sum(everything, axis=0)


def laid_out(tiles, dim):
    tiles = jnp.moveaxis(tiles, 0, dim)
    dims = tiles.shape
    return tiles.reshape(*dims[:dim], dims[dim] * dims[dim + 1], *dims[dim + 2 :])


def gathered_copies(x, axis, dim):
    tiles = sent_to_all(x, axis)
    return laid_out(tiles, dim)


def sent_together(arrays, axis, dim, along):
    ends, at = ([], 0)
    for a in arrays[:-1]:
        at += a.shape[along]
        ends.append(at)
    both = jnp.concatenate(arrays, axis=along)
    return tuple(jnp.split(lax.all_gather(both, axis, axis=dim, tiled=True), ends, axis=along))


def all_blocks(x, axes, sequence):
    tiles = x
    for k in sequence:
        tiles = lax.all_gather(tiles, axes[k])
    done = sequence[::-1]
    back = [done.index(k) for k in range(len(axes))]
    tiles = tiles.transpose(*back, *range(len(axes), tiles.ndim))
    return tiles.reshape(-1, *x.shape)


def gathered_by_axis(x, axes, sequence, dim):
    return laid_out(all_blocks(x, axes, sequence), dim)


def norm_scale(values, gain):
    return values * lax.rsqrt(jnp.mean(values * values, axis=-1, keepdims=True) + EPS) * gain


def conv_three(values, taps):
    height, breadth = values.shape
    grouped = values.reshape(height // SEQ_LEN, SEQ_LEN, breadth)
    padded = jnp.pad(grouped, ((0, 0), (1, 1), (0, 0)))
    mixed = taps[0] * padded[:, :-2] + taps[1] * padded[:, 1:-1] + taps[2] * padded[:, 2:]
    return mixed.reshape(height, breadth)


def settle(partial_value, resid, post_gain):
    share = summed_on_arrival(partial_value.astype(jnp.bfloat16), "tp", 1).astype(jnp.bfloat16)
    share_f = share.astype(jnp.float32)
    breadth = share.shape[1]
    squares = of_everyone(jnp.sum(share_f * share_f, axis=1), "tp")
    factor = lax.rsqrt(squares / (breadth * lax.axis_size("tp")) + EPS)[:, None]
    offset = lax.axis_index("tp") * breadth
    own_cols = lax.dynamic_slice_in_dim(resid, offset, breadth, 1)
    gain_cols = lax.dynamic_slice_in_dim(post_gain, offset, breadth, 0)
    updated = (own_cols + share_f * factor * gain_cols).astype(jnp.bfloat16)
    return gathered_copies(updated, "tp", 1)


def on_device(
    stream,
    mix_pre_gain,
    w_outer_gate,
    w_inner_gate,
    w_value,
    mix_taps,
    w_mix_out,
    mix_post_gain,
    ffn_pre_gain,
    w_linear,
    w_gated,
    ffn_taps,
    ffn_bias,
    w_down,
    ffn_post_gain,
):
    resid = stream.astype(jnp.float32)
    normed = norm_scale(resid, mix_pre_gain).astype(jnp.bfloat16)
    full_outer, full_inner, full_value = sent_together(
        (w_outer_gate, w_inner_gate, w_value), FS, 0, 1
    )
    outer = jnp.dot(normed, full_outer, preferred_element_type=jnp.float32)
    inner = jnp.dot(normed, full_inner, preferred_element_type=jnp.float32)
    value = jnp.dot(normed, full_value, preferred_element_type=jnp.float32)
    outer = outer.astype(jnp.bfloat16)
    inner = inner.astype(jnp.bfloat16)
    value = value.astype(jnp.bfloat16)
    product = inner.astype(jnp.float32) * value.astype(jnp.float32)
    mixed = (outer.astype(jnp.float32) * conv_three(product, mix_taps)).astype(jnp.bfloat16)
    full_mix_out = gathered_copies(w_mix_out, FS, 1)
    partial_value = jnp.dot(mixed, full_mix_out, preferred_element_type=jnp.float32)
    middle = settle(partial_value, resid, mix_post_gain)
    middle_f = middle.astype(jnp.float32)
    normed_two = norm_scale(middle_f, ffn_pre_gain).astype(jnp.bfloat16)
    full_linear, full_gated = sent_together((w_linear, w_gated), FS, 0, 1)
    linear = jnp.dot(normed_two, full_linear, preferred_element_type=jnp.float32)
    gated = jnp.dot(normed_two, full_gated, preferred_element_type=jnp.float32)
    linear = linear.astype(jnp.bfloat16)
    gated = gated.astype(jnp.bfloat16)
    activated = jax.nn.gelu(
        conv_three(gated.astype(jnp.float32), ffn_taps) + ffn_bias, approximate=True
    )
    hidden = (activated * linear.astype(jnp.float32)).astype(jnp.bfloat16)
    full_down = gathered_by_axis(w_down, FS, (0, 1), 1)
    partial_two = jnp.dot(hidden, full_down, preferred_element_type=jnp.float32)
    return settle(partial_two, middle_f, ffn_post_gain)


def solution(mesh):
    split = Mesh(
        mesh.devices.reshape(mesh.shape["rep"], 8, 8, mesh.shape["tp"]),
        ("rep", "fs_0", "fs_1", "tp"),
    )
    return jax.shard_map(
        on_device,
        mesh=split,
        in_specs=(
            P(REP_FS, None),
            P(),
            P(FS, "tp"),
            P(FS, "tp"),
            P(FS, "tp"),
            P(None, "tp"),
            P("tp", FS),
            P(),
            P(),
            P(FS, "tp"),
            P(FS, "tp"),
            P(None, "tp"),
            P("tp"),
            P("tp", FS),
            P(),
        ),
        out_specs=P(REP_FS, None),
        check_vma=False,
    )
```

profile of v0, /device:TPU:1, one launch (start us, length us, event | category | flops | bytes accessed | tf_op | source)
XLA Modules:
  0.0 617.5 jit_solution(11168243926205137896)
XLA Ops:
  6.5 50.5 %all-gather.2 = bf16[8,528,24]{1,2,0:T(8,128)(2,1)} all-gather(bf16[1,528,24]{1,2,0:T(8,128)(2,1)} %bitcast.64), channel_id=2, replica_groups=mesh['rep'=2,'fs_0'=8,'fs_1'=8,'tp'=8] {'fs_0'}, dimensions={0}, use_global_device_ids=true | all-gather | bytes 228096 | tf_op jit(solution)/shard_map/all_gather | solution.py:59
  57.1 1.5 pad_maximum_fusion
  58.6 1.5 broadcast_in_dim.10
  60.1 14.7 %all-to-all-start = ((bf16[64,96,24]{1,2,0:T(8,128)(2,1)}), bf16[64,96,24]{1,2,0:T(8,128)(2,1)S(1)}, u32[]{:S(2)}, u32[]{:S(2)}) async-start(bf16[64,96,24]{1,2,0:T(8,128)(2,1)} %broadcast_in_dim.10), calls=%async_computation | async-start | bytes 786432 | tf_op jit(solution)/shard_map/all_to_all | solution.py:28
  75.4 212.4 %all_gather.18 = bf16[1536,288]{1,0:T(8,128)(2,1)S(1)} all-gather(bf16[24,288]{1,0:T(8,128)(2,1)S(1)} %pad_maximum_fusion.1), channel_id=1, replica_groups=mesh['rep'=2,'fs_0'=8,'fs_1'=8,'tp'=8] {'fs_0','fs_1'}, dimensions={0}, use_global_device_ids=true | all-gather | bytes 898560 | tf_op jit(solution)/shard_map/all_gather | solution.py:53
  287.8 0.8 fusion.24
  290.8 2.0 convolution_convert_fusion.1
  293.1 52.2 %all_to_all.37 = bf16[8,256,192]{1,2,0:T(8,128)(2,1)S(1)} all-to-all(bf16[8,256,192]{1,2,0:T(8,128)(2,1)S(1)} %bitcast.55), channel_id=1, replica_groups=mesh['rep'=2,'fs_0'=8,'fs_1'=8,'tp'=8] {'tp'}, dimensions={0} | all-to-all | bytes 1572864 | tf_op jit(solution)/shard_map/all_to_all | solution.py:22
  346.1 3.9 all-to-all-start.2
  350.1 0.8 dynamic_slice.13
  350.9 4.1 all-to-all-done.2
  355.2 0.9 broadcast_in_dim.12
  356.1 3.7 all-to-all-start.3
  359.9 12.3 %all-to-all-done.3 = bf16[8,256,192]{1,2,0:T(8,128)(2,1)S(1)} async-done(((bf16[8,256,192]{1,2,0:T(8,128)(2,1)}), bf16[8,256,192]{1,2,0:T(8,128)(2,1)S(1)}, u32[]{:S(2)}, u32[]{:S(2)}) %all-to-all-start.3) | async-done | bytes 786464 | tf_op jit(solution)/shard_map/all_to_all | solution.py:28
  372.7 3.4 copy.39
  376.1 132.3 %all-gather.6.cloned.1.call-done = bf16[1536,1056]{1,0:T(8,128)(2,1)} async-done(((bf16[24,1056]{1,0:T(8,128)(2,1)}), bf16[1536,1056]{1,0:T(8,128)(2,1)}) %all-gather.6.cloned.1.call-update) | async-done | bytes 3244048 | tf_op jit(solution)/shard_map/all_gather | solution.py:53
  508.3 3.3 fusion.7
  511.9 3.9 fusion.40
  515.8 4.7 convolution_convert_fusion
  520.8 63.5 %all_to_all.38 = bf16[8,256,192]{1,2,0:T(8,128)(2,1)S(1)} all-to-all(bf16[8,256,192]{1,2,0:T(8,128)(2,1)S(1)} %bitcast.56), channel_id=1, replica_groups=mesh['rep'=2,'fs_0'=8,'fs_1'=8,'tp'=8] {'tp'}, dimensions={0} | all-to-all | bytes 1572864 | tf_op jit(solution)/shard_map/all_to_all | solution.py:22
  585.2 4.3 all-to-all-start.5
  590.2 3.9 all-to-all-done.5
  594.3 15.2 %all_to_all.39 = bf16[8,256,192]{1,2,0:T(8,128)(2,1)S(1)} all-to-all(bf16[8,256,192]{1,2,0:T(8,128)(2,1)S(1)} %broadcast_in_dim.14), channel_id=1, replica_groups=mesh['rep'=2,'fs_0'=8,'fs_1'=8,'tp'=8] {'tp'}, dimensions={0} | all-to-all | bytes 1572864 | tf_op jit(solution)/shard_map/all_to_all | solution.py:28
  609.5 1.2 copy.42
  (58 shorter events, 7.0 us)
Async XLA Ops:
  6.5 68.2 %copy-start = (bf16[256,1536]{1,0:T(8,128)(2,1)S(1)}, bf16[256,1536]{1,0:T(8,128)(2,1)}, u32[]{:S(2)}) copy-start(bf16[256,1536]{1,0:T(8,128)(2,1)} %param.15) | copy-start | bytes 2359300
  6.5 366.2 %all-gather.8.cloned.1.call-start = ((), (), s32[]{:S(2)}) async-start(), calls=%async_computation.8 | async-start | bytes 2211840 | tf_op jit(solution)/shard_map/all_gather | solution.py:59
  57.0 18.1 %copy-start.4 = (bf16[24,96]{1,0:T(8,128)(2,1)S(1)}, bf16[24,96]{1,0:T(8,128)(2,1)}, u32[]{:S(2)}) copy-start(bf16[24,96]{1,0:T(8,128)(2,1)} %param.19) | copy-start | bytes 13828
  57.0 18.1 %copy-start.5 = (bf16[24,96]{1,0:T(8,128)(2,1)S(1)}, bf16[24,96]{1,0:T(8,128)(2,1)}, u32[]{:S(2)}) copy-start(bf16[24,96]{1,0:T(8,128)(2,1)} %param.18) | copy-start | bytes 13828
  57.0 18.1 %copy-start.6 = (bf16[24,96]{1,0:T(8,128)(2,1)S(1)}, bf16[24,96]{1,0:T(8,128)(2,1)}, u32[]{:S(2)}) copy-start(bf16[24,96]{1,0:T(8,128)(2,1)} %param.17) | copy-start | bytes 13828
  57.0 451.3 %all-gather.6.cloned.1.call-start = ((), (), s32[]{:S(2)}) async-start(), calls=%async_computation.7 | async-start | bytes 3594240 | tf_op jit(solution)/shard_map/all_gather | solution.py:53
  60.1 230.0 %all-to-all-start = ((bf16[64,96,24]{1,2,0:T(8,128)(2,1)}), bf16[64,96,24]{1,2,0:T(8,128)(2,1)S(1)}, u32[]{:S(2)}, u32[]{:S(2)}) async-start(bf16[64,96,24]{1,2,0:T(8,128)(2,1)} %broadcast_in_dim.10), calls=%async_computation | async-start | bytes 786432 | tf_op jit(solution)/shard_map/all_to_all | solution.py:28
  74.8 213.0 %copy-start.9 = (f32[1536]{0:T(1024)S(1)}, f32[1536]{0:T(1024)}, u32[]{:S(2)}) copy-start(f32[1536]{0:T(1024)} %param.16) | copy-start | bytes 18436
  288.6 0.9 copy-start.8
  290.1 0.7 copy-start.2
  346.1 8.9 %all-to-all-start.2 = ((f32[8,1,256]{2,1,0:T(1,128)}), f32[8,1,256]{2,1,0:T(1,128)S(1)}, u32[]{:S(2)}, u32[]{:S(2)}) async-start(f32[8,1,256]{2,1,0:T(1,128)} %broadcast_in_dim.11), calls=%async_computation.2 | async-start | bytes 16384 | tf_op jit(solution)/shard_map/all_to_all | solution.py:28
  350.1 9.8 %copy-start.7 = (f32[3,528]{1,0:T(4,128)S(1)}, f32[3,528]{1,0:T(4,128)}, u32[]{:S(2)}) copy-start(f32[3,528]{1,0:T(4,128)} %param.26) | copy-start | bytes 19012
  355.1 17.2 %copy-start.3 = (f32[1536]{0:T(1024)S(1)}, f32[1536]{0:T(1024)}, u32[]{:S(2)}) copy-start(f32[1536]{0:T(1024)} %param.23) | copy-start | bytes 18436
  356.1 16.0 %all-to-all-start.3 = ((bf16[8,256,192]{1,2,0:T(8,128)(2,1)}), bf16[8,256,192]{1,2,0:T(8,128)(2,1)S(1)}, u32[]{:S(2)}, u32[]{:S(2)}) async-start(bf16[8,256,192]{1,2,0:T(8,128)(2,1)} %broadcast_in_dim.12), calls=%async_computation.3 | async-start | bytes 1572864 | tf_op jit(solution)/shard_map/all_to_all | solution.py:28
  372.7 135.7 %copy-start.1 = (bf16[256,1536]{0,1:T(8,128)(2,1)}, bf16[256,1536]{0,1:T(8,128)(2,1)S(1)}, u32[]{:S(2)}) copy-start(bf16[256,1536]{0,1:T(8,128)(2,1)S(1)} %get-tuple-element.8) | copy-start | bytes 2359300
  511.6 4.2 copy-start.10
  585.2 8.9 %all-to-all-start.5 = ((f32[8,1,256]{2,1,0:T(1,128)}), f32[8,1,256]{2,1,0:T(1,128)S(1)}, u32[]{:S(2)}, u32[]{:S(2)}) async-start(f32[8,1,256]{2,1,0:T(1,128)} %broadcast_in_dim.13), calls=%async_computation.5 | async-start | bytes 16384 | tf_op jit(solution)/shard_map/all_to_all | solution.py:28
Sparse Core Ops, SparseCore 0:
  57.1 56.4 all-gather.7
  116.3 392.0 all-gather.5
where the time goes:
time: 618 us
  blocking collectives  394 us (64%)
  waiting for transfers between devices  153 us (25%)
  starting transfers between devices  26.6 us (4%)
  between operations  13.7 us (2%)
  local copies, waits for them, and re-layouts  11.7 us (2%)
  matrix products  11.6 us (2%)
  other arithmetic  7.48 us (1%)
    all_gather x1, blocking collectives, sent_together(): lax.all_gather(both, axis, axis=dim, tiled=True)  212 us
    all_gather x1, waiting for transfers between devices, sent_together(): lax.all_gather(both, axis, axis=dim, tiled=True)  132 us
    all_to_all x2, blocking collectives, summed_on_arrival(): lax.all_to_all(tiles, axis, split_axis=0, concat_axis=0, tiled=True)  116 us
    all_gather x1, blocking collectives, all_blocks(): tiles = lax.all_gather(tiles, axes[k])  50.5 us
    all_to_all x4, starting transfers between devices, sent_to_all(): lax.all_to_all(jnp.broadcast_to(x[None], (length, *x.shape)), axis, 0, 0,...  26.6 us
    all_to_all x4, waiting for transfers between devices, sent_to_all(): lax.all_to_all(jnp.broadcast_to(x[None], (length, *x.shape)), axis, 0, 0,...  20.3 us
    all_to_all x1, blocking collectives, sent_to_all(): lax.all_to_all(jnp.broadcast_to(x[None], (length, *x.shape)), axis, 0, 0,...  15.2 us
  transfers between devices with their start and end apart: 6, of which 4 were waited for; matrix products, arithmetic and copies ran while one was open for 2% of the time, Pallas kernels for 0%

commit v1 on v0

v1 whole, which is shorter than its diff:
```python
import jax
import jax.numpy as jnp
from jax import lax
from jax.sharding import Mesh
from jax.sharding import PartitionSpec as P

SEQ_LEN = 128
FS = ("fs_0", "fs_1")
REP_FS = ("rep", "fs_0", "fs_1")
EPS = 1e-06
F32 = jnp.float32
BF16 = jnp.bfloat16


def of_reps(first, second):
    return jnp.where(lax.axis_index("rep") == 0, first, second)


def plane_gathered(first, second):
    mine = of_reps(first, second)
    both = lax.all_gather(mine, REP_FS, axis=0, tiled=True)
    rows = both.shape[0] // 2
    return both[:rows], both[rows:]


def norm_scale(values, gain):
    return values * lax.rsqrt(jnp.mean(values * values, axis=-1, keepdims=True) + EPS) * gain


def conv_three(values, taps):
    height, breadth = values.shape
    grouped = values.reshape(height // SEQ_LEN, SEQ_LEN, breadth)
    padded = jnp.pad(grouped, ((0, 0), (1, 1), (0, 0)))
    mixed = taps[0] * padded[:, :-2] + taps[1] * padded[:, 1:-1] + taps[2] * padded[:, 2:]
    return mixed.reshape(height, breadth)


def dot(a, b):
    return jnp.dot(a, b, preferred_element_type=F32)


def dot_t(a, b):
    return lax.dot_general(a, b, (((1,), (1,)), ((), ())), preferred_element_type=F32)


def rows_summed(partial_value):
    n = lax.axis_size("tp")
    tiles = partial_value.astype(BF16).reshape(n, -1, partial_value.shape[1])
    arrived = lax.all_to_all(tiles, "tp", split_axis=0, concat_axis=0, tiled=True)
    return arrived.astype(F32).sum(axis=0).astype(BF16).astype(F32)


def rows_gathered(x):
    n = lax.axis_size("tp")
    tiles = lax.all_to_all(jnp.broadcast_to(x[None], (n, *x.shape)), "tp", 0, 0, tiled=True)
    return tiles.reshape(-1, x.shape[1])


def on_device(
    stream,
    mix_pre_gain,
    w_outer_gate,
    w_inner_gate,
    w_value,
    mix_taps,
    w_mix_out,
    mix_post_gain,
    ffn_pre_gain,
    w_linear,
    w_gated,
    ffn_taps,
    ffn_bias,
    w_down,
    ffn_post_gain,
):
    width = w_value.shape[1]
    hidden_w = w_linear.shape[1]
    split = hidden_w // 256 * 128
    tail = hidden_w - 2 * split
    down_t = w_down.T
    first_mix, second_mix = plane_gathered(
        jnp.concatenate([w_outer_gate, w_inner_gate], axis=1),
        jnp.concatenate([w_value, w_mix_out.T], axis=1),
    )
    down_tail = down_t[:, 2 * split :]
    first_up, second_up = plane_gathered(
        jnp.concatenate([w_linear, down_tail], axis=1),
        jnp.concatenate([w_gated, down_tail], axis=1),
    )
    first_down, second_down = plane_gathered(down_t[:, :split], down_t[:, split : 2 * split])

    resid = stream.astype(F32)
    normed = norm_scale(resid, mix_pre_gain).astype(BF16)
    outer_inner = dot(normed, first_mix).astype(BF16).astype(F32)
    outer, inner = outer_inner[:, :width], outer_inner[:, width:]
    value = dot(normed, second_mix[:, :width]).astype(BF16).astype(F32)
    mixed = (outer * conv_three(inner * value, mix_taps)).astype(BF16)
    branch = rows_summed(dot_t(mixed, second_mix[:, width:]))
    rows = branch.shape[0]
    own = lax.dynamic_slice_in_dim(stream, lax.axis_index("tp") * rows, rows, 0).astype(F32)
    middle = (own + norm_scale(branch, mix_post_gain)).astype(BF16).astype(F32)
    normed_two = rows_gathered(norm_scale(middle, ffn_pre_gain).astype(BF16))

    linear = dot(normed_two, first_up[:, :hidden_w]).astype(BF16).astype(F32)
    gated = dot(normed_two, second_up[:, :hidden_w]).astype(BF16).astype(F32)
    activated = jax.nn.gelu(conv_three(gated, ffn_taps) + ffn_bias, approximate=True)
    hidden = (activated * linear).astype(BF16)
    partial_two = dot_t(hidden[:, :split], first_down)
    partial_two += dot_t(hidden[:, split : 2 * split], second_down)
    partial_two += dot_t(hidden[:, 2 * split :], first_up[:, hidden_w : hidden_w + tail])
    branch_two = rows_summed(partial_two)
    return rows_gathered((middle + norm_scale(branch_two, ffn_post_gain)).astype(BF16))


def solution(mesh):
    split = Mesh(
        mesh.devices.reshape(mesh.shape["rep"], 8, 8, mesh.shape["tp"]),
        ("rep", "fs_0", "fs_1", "tp"),
    )
    return jax.shard_map(
        on_device,
        mesh=split,
        in_specs=(
            P(REP_FS, None),
            P(),
            P(FS, "tp"),
            P(FS, "tp"),
            P(FS, "tp"),
            P(None, "tp"),
            P("tp", FS),
            P(),
            P(),
            P(FS, "tp"),
            P(FS, "tp"),
            P(None, "tp"),
            P("tp"),
            P("tp", FS),
            P(),
        ),
        out_specs=P(REP_FS, None),
        check_vma=False,
    )
```

time: 618 us -> 509 us (0.82)
  blocking collectives: 394 us -> 42.7 us
  waiting for transfers between devices: 153 us -> 407 us
  local copies, waits for them, and re-layouts: 11.7 us -> 3.79 us
  starting transfers between devices: 26.6 us -> 19.8 us
    all_gather x2 -> x0, blocking collectives: 263 us -> none  [the longest x1 212 us: sent_together(): lax.all_gather(both, axis, axis=dim, tiled=True)]
    all_gather x2 -> x3, waiting for transfers between devices: 132 us -> 383 us  [plane_gathered(): both = lax.all_gather(mine, REP_FS, axis=0, tiled=True)]
    all_to_all x3 -> x2, blocking collectives: 131 us -> 42.7 us  [the longest x1 27.1 us: rows_summed(): lax.all_to_all(tiles, 'tp', split_axis=0, concat_axis=0, tiled=True)]
    all_to_all x4 -> x2, starting transfers between devices: 26.6 us -> 19.7 us  [the longest x1 15.3 us: rows_summed(): lax.all_to_all(tiles, 'tp', split_axis=0, concat_axis=0, tiled=True)]
    all_to_all x4 -> x2, waiting for transfers between devices: 20.3 us -> 23.6 us  [the longest x1 12.2 us: rows_gathered(): lax.all_to_all(jnp.broadcast_to(x[None], (n, *x.shape)), 'tp', 0, 0, tile...]
  transfers between devices with their start and end apart: 6 -> 5, of which waited for: 4 -> 5; matrix products, arithmetic and copies ran while one was open for 2% -> 4% of each run, Pallas kernels for 0% -> 0%
where the time goes in v1:
time: 509 us; the launch traced here: 508 us
  waiting for transfers between devices  407 us (80%)
  blocking collectives  42.7 us (8%)
  starting transfers between devices  19.8 us (4%)
  between operations  13.3 us (3%)
  matrix products  12.3 us (2%)
  other arithmetic  9.66 us (2%)
    all_gather x3, waiting for transfers between devices, plane_gathered(): both = lax.all_gather(mine, REP_FS, axis=0, tiled=True)  383 us
    all_to_all x1, blocking collectives, rows_summed(): lax.all_to_all(tiles, 'tp', split_axis=0, concat_axis=0, tiled=True)  27.1 us
    all_to_all x1, blocking collectives, rows_gathered(): lax.all_to_all(jnp.broadcast_to(x[None], (n, *x.shape)), 'tp', 0, 0, tile...  15.6 us
    all_to_all x1, starting transfers between devices, rows_summed(): lax.all_to_all(tiles, 'tp', split_axis=0, concat_axis=0, tiled=True)  15.3 us
    all_to_all x1, waiting for transfers between devices, rows_gathered(): lax.all_to_all(jnp.broadcast_to(x[None], (n, *x.shape)), 'tp', 0, 0, tile...  12.2 us
    all_to_all x1, waiting for transfers between devices, rows_summed(): lax.all_to_all(tiles, 'tp', split_axis=0, concat_axis=0, tiled=True)  11.4 us
  transfers between devices with their start and end apart: 5, of which 5 were waited for; matrix products, arithmetic and copies ran while one was open for 4% of the time, Pallas kernels for 0%

profile of v1, /device:TPU:1, one launch (start us, length us, event | category | flops | bytes accessed | tf_op | source)
XLA Modules:
  0.0 508.1 jit_solution(3411715988286173963)
XLA Ops:
  6.5 1.4 maximum_select_fusion
  8.0 0.7 slice.119
  8.7 1.4 fusion.67
  10.2 1.4 fusion.5
  11.7 0.8 slice_bitcast_fusion.2
  12.5 145.1 %all-gather.4.cloned.1.call-done = bf16[3072,192]{1,0:T(8,128)(2,1)} async-done(((bf16[24,192]{1,0:T(8,128)(2,1)}), bf16[3072,192]{1,0:T(8,128)(2,1)}) %all-gather.4.cloned.1.call-update) | async-done | bytes 1179664 | tf_op jit(solution)/shard_map/all_gather | solution.py:21
  157.6 2.0 fusion.26
  160.8 1.4 convolution_convert_fusion
  162.2 15.3 %all-to-all-start = ((bf16[8,32,1536]{2,1,0:T(8,128)(2,1)}), bf16[8,32,1536]{2,1,0:T(8,128)(2,1)S(1)}, u32[]{:S(2)}, u32[]{:S(2)}) async-start(bf16[8,32,1536]{2,1,0:T(8,128)(2,1)} %bitcast.4), calls=%async_computation | async-start | bytes 1572864 | tf_op jit(solution)/shard_map/all_to_all | solution.py:49
  177.5 0.6 slice_select_fusion
  178.2 11.4 %all-to-all-done = bf16[8,32,1536]{2,1,0:T(8,128)(2,1)S(1)} async-done(((bf16[8,32,1536]{2,1,0:T(8,128)(2,1)}), bf16[8,32,1536]{2,1,0:T(8,128)(2,1)S(1)}, u32[]{:S(2)}, u32[]{:S(2)}) %all-to-all-start) | async-done | bytes 786464 | tf_op jit(solution)/shard_map/all_to_all | solution.py:49
  190.3 0.9 broadcast_in_dim.4
  191.2 4.4 all-to-all-start.1
  195.7 12.2 %all-to-all-done.1 = bf16[8,32,1536]{2,1,0:T(8,128)(2,1)S(1)} async-done(((bf16[8,32,1536]{2,1,0:T(8,128)(2,1)}), bf16[8,32,1536]{2,1,0:T(8,128)(2,1)S(1)}, u32[]{:S(2)}, u32[]{:S(2)}) %all-to-all-start.1) | async-done | bytes 786464 | tf_op jit(solution)/shard_map/all_to_all | solution.py:55
  207.8 100.8 %all-gather.6.cloned.1.call-done = bf16[3072,544]{1,0:T(8,128)(2,1)} async-done(((bf16[24,544]{1,0:T(8,128)(2,1)}), bf16[3072,544]{1,0:T(8,128)(2,1)}) %all-gather.6.cloned.1.call-update) | async-done | bytes 3342352 | tf_op jit(solution)/shard_map/all_gather | solution.py:21
  308.7 2.4 fusion.11
  311.3 3.2 fusion.42
  314.6 2.5 fusion.23
  317.1 136.8 %all-gather.8.cloned.1.call-done = bf16[3072,256]{1,0:T(8,128)(2,1)} async-done(((bf16[24,256]{1,0:T(8,128)(2,1)}), bf16[3072,256]{1,0:T(8,128)(2,1)}) %all-gather.8.cloned.1.call-update) | async-done | bytes 1572880 | tf_op jit(solution)/shard_map/all_gather | solution.py:21
  453.9 1.7 fusion.30
  456.0 1.5 fusion
  457.5 27.1 %all_to_all.20 = bf16[8,32,1536]{2,1,0:T(8,128)(2,1)S(1)} all-to-all(bf16[8,32,1536]{2,1,0:T(8,128)(2,1)S(1)} %bitcast.34), channel_id=1, replica_groups=mesh['rep'=2,'fs_0'=8,'fs_1'=8,'tp'=8] {'tp'}, dimensions={0} | all-to-all | bytes 1572864 | tf_op jit(solution)/shard_map/all_to_all | solution.py:49
  485.1 15.6 %all_to_all.21 = bf16[8,32,1536]{2,1,0:T(8,128)(2,1)S(1)} all-to-all(bf16[8,32,1536]{2,1,0:T(8,128)(2,1)S(1)} %broadcast_in_dim.5), channel_id=1, replica_groups=mesh['rep'=2,'fs_0'=8,'fs_1'=8,'tp'=8] {'tp'}, dimensions={0} | all-to-all | bytes 1572864 | tf_op jit(solution)/shard_map/all_to_all | solution.py:55
  500.7 0.9 copy.22
  (44 shorter events, 3.0 us)
Async XLA Ops:
  6.5 151.1 %all-gather.4.cloned.1.call-start = ((), (), s32[]{:S(2)}) async-start(), calls=%async_computation.4 | async-start | bytes 1585152 | tf_op jit(solution)/shard_map/all_gather | solution.py:21
  8.0 300.7 %all-gather.6.cloned.1.call-start = ((), (), s32[]{:S(2)}) async-start(), calls=%async_computation.5 | async-start | bytes 3962880 | tf_op jit(solution)/shard_map/all_gather | solution.py:21
  10.2 149.4 %copy-start.1 = (bf16[256,1536]{1,0:T(8,128)(2,1)S(1)}, bf16[256,1536]{1,0:T(8,128)(2,1)}, u32[]{:S(2)}) copy-start(bf16[256,1536]{1,0:T(8,128)(2,1)} %param.15) | copy-start | bytes 2359300
  10.2 149.4 %copy-start.8 = (f32[1536]{0:T(1024)S(1)}, f32[1536]{0:T(1024)}, u32[]{:S(2)}) copy-start(f32[1536]{0:T(1024)} %param.16) | copy-start | bytes 18436
  157.6 2.0 copy-start.2
  160.2 17.3 %copy-start.3 = (bf16[528,24]{0,1:T(8,128)(2,1)S(1)}, bf16[528,24]{0,1:T(8,128)(2,1)}, u32[]{:S(2)}) copy-start(bf16[528,24]{0,1:T(8,128)(2,1)} %param.28) | copy-start | bytes 76036
  162.2 27.7 %copy-start.4 = (f32[1536]{0:T(1024)S(1)}, f32[1536]{0:T(1024)}, u32[]{:S(2)}) copy-start(f32[1536]{0:T(1024)} %param.22) | copy-start | bytes 18436
  162.2 28.0 %copy-start.5 = (f32[1536]{0:T(1024)S(1)}, f32[1536]{0:T(1024)}, u32[]{:S(2)}) copy-start(f32[1536]{0:T(1024)} %param.23) | copy-start | bytes 18436
  162.2 27.5 %all-to-all-start = ((bf16[8,32,1536]{2,1,0:T(8,128)(2,1)}), bf16[8,32,1536]{2,1,0:T(8,128)(2,1)S(1)}, u32[]{:S(2)}, u32[]{:S(2)}) async-start(bf16[8,32,1536]{2,1,0:T(8,128)(2,1)} %bitcast.4), calls=%async_computation | async-start | bytes 1572864 | tf_op jit(solution)/shard_map/all_to_all | solution.py:49
  177.5 276.4 %all-gather.8.cloned.1.call-start = ((), (), s32[]{:S(2)}) async-start(), calls=%async_computation.6 | async-start | bytes 1585152 | tf_op jit(solution)/shard_map/all_gather | solution.py:21
  189.8 5.9 %copy-start.7 = (f32[3,528]{1,0:T(4,128)S(1)}, f32[3,528]{1,0:T(4,128)}, u32[]{:S(2)}) copy-start(f32[3,528]{1,0:T(4,128)} %param.26) | copy-start | bytes 19012
  191.2 16.6 %all-to-all-start.1 = ((bf16[8,32,1536]{2,1,0:T(8,128)(2,1)}), bf16[8,32,1536]{2,1,0:T(8,128)(2,1)S(1)}, u32[]{:S(2)}, u32[]{:S(2)}) async-start(bf16[8,32,1536]{2,1,0:T(8,128)(2,1)} %broadcast_in_dim.4), calls=%async_computation.1 | async-start | bytes 1572864 | tf_op jit(solution)/shard_map/all_to_all | solution.py:55
  311.0 3.5 copy-start.9
  453.9 1.7 copy-start
  457.5 27.4 %copy-start.6 = (f32[1536]{0:T(1024)S(1)}, f32[1536]{0:T(1024)}, u32[]{:S(2)}) copy-start(f32[1536]{0:T(1024)} %param.29) | copy-start | bytes 18436
Sparse Core Ops, SparseCore 0:
  11.5 146.0 all-gather.3
  161.7 146.8 all-gather.5
  312.8 141.0 all-gather.7
